TPU v7x, 512 devices: a whole 4x4x16 slice. The times are simulated.
512 devices in a mesh: ep: 32 (over z, core), tp: 16 (over y, x).
Axes of the slice: x: 4, y: 4, z: 16, core: 2. Of those that a mesh axis runs over, the one named last changes fastest.
Arguments:
- queries: bfloat16 [8192, 2048], P('ep', 'tp'), may hold values from -6 to 6
- key_rows: bfloat16 [8192, 1024], P('ep', 'tp'), may hold values from -6 to 6
- values: bfloat16 [8192, 1024], P('ep', 'tp'), may hold values from -140 to 140
- query_gain: float32 [64], replicated, may hold values from 0.55 to 7.5
- key_gain: float32 [64], replicated, may hold values from 0.55 to 7.5
- mix_gain: float32 [2048], replicated, may hold values from 0.1 to 1.9
- out_weight: bfloat16 [2048, 4096], P(None, 'tp'), may hold values from -0.125 to 0.125
- expert_input: bfloat16 [8192, 4096], P('ep', 'tp'), may hold values from -140 to 140
- expert_gain: float32 [4096], replicated, may hold values from 0.1 to 1.9
- route_ids: int32 [8192, 2], P('ep'), may hold values from 0 to 31, as said below
- route_weights: float32 [8192, 2], P('ep'), may hold values from 0.3 to 1.7
- expert_gate: bfloat16 [32, 4096, 2048], P('ep', None, 'tp'), may hold values from -0.09375 to 0.09375
- expert_up: bfloat16 [32, 4096, 2048], P('ep', None, 'tp'), may hold values from -0.09375 to 0.09375
- expert_down: bfloat16 [32, 2048, 4096], P('ep', None, 'tp'), may hold values from -0.125 to 0.125
Outputs:
- attended: bfloat16 [8192, 4096], P('ep', 'tp')
- expert_mix: bfloat16 [8192, 4096], P('ep', 'tp')
Inputs may be any that keep to these rules, and one draw needn't show every extreme that they name: `route_ids`: the 2 experts of a row differ. In every aligned block of 256 rows no expert is named more than 22 times, and one expert, the same for all blocks, is named exactly 22 times in every block.
All inputs are finite; a program needn't handle non-finite values.
Results may differ from a plain program's by a relative error of at most 0.01.
The roundings to bfloat16 on the way count: a program that leaves them out, or rounds other values in their place, can miss the bound.
Values may be sent and summed in bfloat16 or wider, within the bound.
A program may use at most 64 MiB of HBM per device.

v0:
```python
import math
import jax
import jax.numpy as jnp
from jax import lax
from jax.sharding import Mesh
from jax.sharding import PartitionSpec as P

Q_HEADS = 32
KV_HEADS = 16
HEAD = 64
GRID_W = 64
EP = ("ep_0", "ep_1")
EPS = 1e-06
THETA = 10000.0


def in_one_piece(arrays, axis, dim, along):
    widths = [a.shape[along] for a in arrays]
    both = jnp.concatenate(arrays, axis=along)
    filled = lax.all_gather(both, axis, axis=dim, tiled=True)
    return tuple(jnp.split(filled, [sum(widths[:k]) for k in range(1, len(widths))], axis=along))


def split_up(array, dim, length):
    before, after = (array.shape[:dim], array.shape[dim + 1 :])
    return jnp.moveaxis(array.reshape(*before, length, -1, *after), dim, 0)


def joined_along(blocks, dim):
    lengths = list(blocks.shape[1:])
    lengths[dim] *= blocks.shape[0]
    return jnp.moveaxis(blocks, 0, dim).reshape(lengths)


def exchange_in_order(blocks, axes, order):
    inside = blocks.shape[1:]
    filled = blocks.reshape(*(lax.axis_size(a) for a in axes), *inside)
    for k in order:
        filled = lax.all_to_all(filled, axes[k], k, k, tiled=True)
    return filled.reshape(-1, *inside)


def exchange_by_chip(array, groups, order, split_dim, concat_dim):
    length = lax.axis_size(groups[0]) * lax.axis_size(groups[1])
    blocks = split_up(array, split_dim, length)
    return joined_along(exchange_in_order(blocks, groups, order), concat_dim)


def turn_tables(offset, length):
    half_width = HEAD // 2
    inverse = THETA ** (-jnp.arange(0, half_width, 2, dtype=jnp.float32) / half_width)
    positions = offset + jnp.arange(length, dtype=jnp.int32)
    grid_rows = (positions // GRID_W).astype(jnp.float32)
    grid_cols = (positions % GRID_W).astype(jnp.float32)
    angles = jnp.concatenate([grid_rows[:, None] * inverse, grid_cols[:, None] * inverse], axis=-1)
    return (jnp.cos(angles), jnp.sin(angles))


def norm_turn(source, scale_gain, cosine_table, sine_table):
    length = source.shape[0]
    head_rows = source.astype(jnp.float32).reshape(length, -1, HEAD)
    head_rows = (
        head_rows
        * lax.rsqrt(jnp.mean(head_rows * head_rows, axis=-1, keepdims=True) + EPS)
        * scale_gain
    )
    pair_view = head_rows.reshape(length, head_rows.shape[1], HEAD // 2, 2)
    even_part = pair_view[..., 0]
    odd_part = pair_view[..., 1]
    cosine_part = cosine_table[:, None, :]
    sine_part = sine_table[:, None, :]
    turned = jnp.stack(
        [
            even_part * cosine_part - odd_part * sine_part,
            even_part * sine_part + odd_part * cosine_part,
        ],
        axis=-1,
    )
    return turned.reshape(length, -1).astype(jnp.bfloat16)


def shards(
    queries,
    key_rows,
    values,
    query_gain,
    key_gain,
    mix_gain,
    out_weight,
    expert_input,
    expert_gain,
    route_ids,
    route_weights,
    expert_gate,
    expert_up,
    expert_down,
):
    length = queries.shape[0]
    experts_count = lax.axis_size(EP)
    offset = lax.axis_index(EP) * length
    cosine_table, sine_table = turn_tables(offset, length)
    query_turned = norm_turn(queries, query_gain, cosine_table, sine_table)
    key_turned = norm_turn(key_rows, key_gain, cosine_table, sine_table)
    kv_local = key_rows.shape[1] // HEAD
    group_size = Q_HEADS // KV_HEADS
    query_heads = query_turned.reshape(length, kv_local, group_size, HEAD)
    start_state = (
        jnp.full((kv_local, group_size, length), -jnp.inf, jnp.float32),
        jnp.zeros((kv_local, group_size, length), jnp.float32),
        jnp.zeros((length, kv_local, group_size, HEAD), jnp.float32),
    )
    key_piece, value_piece = in_one_piece((key_turned, values), EP, 0, 1)
    piece_rows = key_piece.shape[0]
    step_rows = 1024
    key_blocks = key_piece.reshape(piece_rows // step_rows, step_rows, kv_local, HEAD)
    value_blocks = value_piece.reshape(piece_rows // step_rows, step_rows, kv_local, HEAD)

    def absorb(current, block_pair):
        running_max, running_sum, running_acc = current
        key_block, value_block = block_pair
        scores = jnp.einsum(
            "rhgd,nhd->hgrn", query_heads, key_block, preferred_element_type=jnp.float32
        ) / math.sqrt(HEAD)
        new_max = jnp.maximum(running_max, jnp.max(scores, axis=-1))
        factor = jnp.exp(running_max - new_max)
        raw_weights = jnp.exp(scores - new_max[..., None])
        new_sum = running_sum * factor + jnp.sum(raw_weights, axis=-1)
        rounded = raw_weights.astype(jnp.bfloat16)
        increment = jnp.einsum(
            "hgrn,nhd->rhgd", rounded, value_block, preferred_element_type=jnp.float32
        )
        new_acc = running_acc * jnp.transpose(factor, (2, 0, 1))[..., None] + increment
        return ((new_max, new_sum, new_acc), None)

    result, unused = lax.scan(absorb, start_state, (key_blocks, value_blocks))
    heads_out = (
        (result[2] / jnp.transpose(result[1], (2, 0, 1))[..., None])
        .reshape(length, -1)
        .astype(jnp.bfloat16)
    )
    top_count = route_ids.shape[1]
    copies = route_ids.shape[0] * top_count
    capacity = (4 * copies + 3 * experts_count - 1) // (3 * experts_count)
    slot_total = experts_count * capacity
    flat_ids = route_ids.reshape(copies)
    hit_marks = (flat_ids[:, None] == jnp.arange(experts_count, dtype=jnp.int32)[None, :]).astype(
        jnp.int32
    )
    earlier = jnp.cumsum(hit_marks, axis=0) - hit_marks
    places = jnp.sum(earlier * hit_marks, axis=1)
    slot_index = flat_ids * capacity + places
    slot_rows = (
        jnp.full((slot_total,), route_ids.shape[0], jnp.int32)
        .at[slot_index]
        .set(jnp.arange(copies, dtype=jnp.int32) // top_count)
    )
    width_local = expert_input.shape[1]
    padded = jnp.concatenate([expert_input, jnp.zeros((1, width_local), jnp.bfloat16)], axis=0)
    outgoing = padded[slot_rows].reshape(experts_count, capacity, width_local)
    arrived = exchange_by_chip(outgoing, ("ep_0", "ep_1"), (1, 0), 0, 0).reshape(
        slot_total, width_local
    )
    piece_float = lax.all_gather(arrived, "tp", axis=1, tiled=True).astype(jnp.float32)
    gain_piece = expert_gain
    scaled_piece = (piece_float * gain_piece).astype(jnp.bfloat16)
    gate_rows = expert_gate[0]
    up_rows = expert_up[0]
    gate_sum = jnp.dot(scaled_piece, gate_rows, preferred_element_type=jnp.float32)
    up_sum = jnp.dot(scaled_piece, up_rows, preferred_element_type=jnp.float32)
    square_sum = jnp.sum(piece_float * piece_float, axis=1)
    row_stat = lax.rsqrt(square_sum / expert_gain.shape[0] + EPS)
    gate_value = gate_sum * row_stat[:, None]
    up_value = up_sum * row_stat[:, None]
    hidden = (jax.nn.silu(gate_value) * up_value).astype(jnp.bfloat16)
    width_out = out_weight.shape[1]
    head_piece, hidden_piece = in_one_piece((heads_out, hidden), "tp", 1, 0)
    head_float = head_piece.astype(jnp.float32)
    gain_piece = mix_gain
    mix_in = (head_float * gain_piece).astype(jnp.bfloat16)
    down_rows = expert_down[0]
    mix_sum = jnp.dot(mix_in, out_weight, preferred_element_type=jnp.float32)
    mix_squares = jnp.sum(head_float * head_float, axis=1)
    expert_sum = jnp.dot(hidden_piece, down_rows, preferred_element_type=jnp.float32)
    attended = (mix_sum * lax.rsqrt(mix_squares / mix_gain.shape[0] + EPS)[:, None]).astype(
        jnp.bfloat16
    )
    expert_back = expert_sum.astype(jnp.bfloat16).reshape(experts_count, capacity, width_out)
    returned = lax.all_to_all(expert_back, EP, split_axis=0, concat_axis=0, tiled=True).reshape(
        slot_total, width_out
    )
    picked = returned[slot_index].astype(jnp.float32) * route_weights.reshape(copies)[:, None]
    expert_mix = jnp.sum(picked.reshape(route_ids.shape[0], top_count, width_out), axis=1).astype(
        jnp.bfloat16
    )
    return (attended, expert_mix)


def solution(mesh):
    torus = Mesh(mesh.devices.reshape(16, 2, mesh.shape["tp"]), ("ep_0", "ep_1", "tp"))
    return jax.shard_map(
        shards,
        mesh=torus,
        in_specs=(
            P(EP, "tp"),
            P(EP, "tp"),
            P(EP, "tp"),
            P(),
            P(),
            P(),
            P(None, "tp"),
            P(EP, "tp"),
            P(),
            P(EP, None),
            P(EP, None),
            P(EP, None, "tp"),
            P(EP, None, "tp"),
            P(EP, None, "tp"),
        ),
        out_specs=(P(EP, "tp"), P(EP, "tp")),
        check_vma=False,
    )
```

profile of v0, /device:TPU:1, one launch (start us, length us, event | category | flops | bytes accessed | tf_op | source)
XLA Modules:
  0.0 310.1 jit_solution(1185379400146651329)
XLA Ops:
  9.4 1.4 pad_maximum_fusion.1
  15.4 2.4 scatter_custom_fusion
  17.9 2.8 gather_fusion
  20.9 10.5 %all_to_all.15 = bf16[16,2,1,22,256]{4,0,3,2,1:T(8,128)(2,1)S(1)} all-to-all(bf16[16,2,1,22,256]{4,0,3,2,1:T(8,128)(2,1)S(1)} %copy.45), channel_id=1, replica_groups=mesh['ep_0'=16,'ep_1'=2,'tp'=16] {'ep_1'}, dimensions={1} | all-to-all | bytes 720896 | tf_op jit(solution)/shard_map/all_to_all | solution.py:39
  32.5 9.6 %all-to-all-start.1 = ((bf16[16,2,1,22,256]{4,1,3,2,0:T(2,128)(2,1)}), bf16[16,2,1,22,256]{4,1,3,2,0:T(2,128)(2,1)S(1)}, u32[]{:S(2)}, u32[]{:S(2)}) async-start(bf16[16,2,1,22,256]{4,1,3,2,0:T(2,128)(2,1)} %copy.46), calls=%async_computation.1 | async-start | bytes 720896 | tf_op jit(solution)/shard_map/all_to_all | solution.py:39
  43.2 20.0 %all-to-all-done.1 = bf16[16,2,1,22,256]{4,1,3,2,0:T(2,128)(2,1)S(1)} async-done(((bf16[16,2,1,22,256]{4,1,3,2,0:T(2,128)(2,1)}), bf16[16,2,1,22,256]{4,1,3,2,0:T(2,128)(2,1)S(1)}, u32[]{:S(2)}, u32[]{:S(2)}) %all-to-all-start.1) | async-done | bytes 360480 | tf_op jit(solution)/shard_map/all_to_all | solution.py:39
  64.3 35.3 %all-gather.4.cloned.1.call-done = bf16[8192,128]{0,1:T(8,128)(2,1)} async-done(((bf16[256,128]{0,1:T(8,128)(2,1)}), bf16[8192,128]{0,1:T(8,128)(2,1)}) %all-gather.4.cloned.1.call-update) | async-done | bytes 2097168 | tf_op jit(solution)/shard_map/all_gather | solution.py:20
  99.5 1.7 fusion.70
  101.8 1.6 copy.39
  104.0 1.5 copy.40
  105.5 25.7 %while.15 = (s32[]{:T(128)}, f32[1,2,256]{2,1,0:T(2,128)S(1)}, f32[1,2,256]{2,1,0:T(2,128)S(1)}, f32[256,1,2,64]{0,3,2,1:T(8,128)S(1)}, bf16[8,1024,1,64]{1,3,2,...) while((s32[]{:T(128)}, f32[1,2,256]{2,1,0:T(2,128)S(1)}, ...), condition=%wide.region_5.6_spmd.clone, body=%wide.region_2.5_spmd.clone.sunk | while | flops 138513408 | bytes 6914169 | solution.py:135
  113.7 1.4 fusion.82
  120.2 1.4 fusion.82
  131.4 42.5 %all-gather.6.cloned.1.call-done = bf16[704,4096]{1,0:T(8,128)(2,1)} async-done(((bf16[704,256]{1,0:T(8,128)(2,1)}), bf16[704,4096]{1,0:T(8,128)(2,1)}) %all-gather.6.cloned.1.call-update) | async-done | bytes 5767184 | tf_op jit(solution)/shard_map/all_gather | solution.py:163
  173.9 4.0 %fusion.19 = f32[704]{0:T(1024)S(1)} fusion(bf16[704,4096]{1,0:T(8,128)(2,1)} %all-gather.6.cloned.1.call-done), kind=kLoop, calls=%fused_computation.32 | loop fusion | flops 8650048 | bytes 5769984 | tf_op jit(solution)/shard_map/reduce_sum | solution.py:170
  178.2 3.0 fusion.31
  181.2 1.7 fusion.40
  183.7 70.5 %all-gather.8.cloned.1.call-done = bf16[960,2048]{1,0:T(8,128)(2,1)} async-done(((bf16[960,128]{1,0:T(8,128)(2,1)}), bf16[960,2048]{1,0:T(8,128)(2,1)}) %all-gather.8.cloned.1.call-update) | async-done | bytes 3932176 | tf_op jit(solution)/shard_map/all_gather | solution.py:20
  254.2 2.7 fusion.28
  257.8 14.4 %all-to-all-start.2 = ((bf16[32,22,256]{2,1,0:T(8,128)(2,1)}), bf16[32,22,256]{2,1,0:T(8,128)(2,1)S(1)}, u32[]{:S(2)}, u32[]{:S(2)}) async-start(bf16[32,22,256]{2,1,0:T(8,128)(2,1)} %reshape.435), calls=%async_computation.2 | async-start | bytes 786432 | tf_op jit(solution)/shard_map/all_to_all | solution.py:188
  272.3 1.5 fusion.27
  273.8 2.3 fusion.43
  276.2 23.7 %all-to-all-done.2 = bf16[32,22,256]{2,1,0:T(8,128)(2,1)S(1)} async-done(((bf16[32,22,256]{2,1,0:T(8,128)(2,1)}), bf16[32,22,256]{2,1,0:T(8,128)(2,1)S(1)}, u32[]{:S(2)}, u32[]{:S(2)}) %all-to-all-start.2) | async-done | bytes 360480 | tf_op jit(solution)/shard_map/all_to_all | solution.py:188
  300.0 2.0 gather_fusion.1
  (130 shorter events, 37.8 us)
Async XLA Ops:
  7.2 247.0 %copy-start = (bf16[1,2048,256]{2,1,0:T(8,128)(2,1)S(1)}, bf16[1,2048,256]{2,1,0:T(8,128)(2,1)}, u32[]{:S(2)}) copy-start(bf16[1,2048,256]{2,1,0:T(8,128)(2,1)} %param.29) | copy-start | bytes 3145732
  7.2 92.3 %all-gather.4.cloned.1.call-start = ((), (), s32[]{:S(2)}) async-start(), calls=%async_computation.3 | async-start | bytes 2162688 | tf_op jit(solution)/shard_map/all_gather | solution.py:20
  17.9 24.3 %copy-start.2 = (bf16[256,128]{1,0:T(8,128)(2,1)S(1)}, bf16[256,128]{1,0:T(8,128)(2,1)}, u32[]{:S(2)}) copy-start(bf16[256,128]{1,0:T(8,128)(2,1)} %param.16) | copy-start | bytes 196612
  17.9 24.5 %copy-start.4 = (f32[64]{0:T(128)S(1)}, f32[64]{0:T(128)}, u32[]{:S(2)}) copy-start(f32[64]{0:T(128)} %param.19) | copy-start | bytes 772
  32.5 30.6 %all-to-all-start.1 = ((bf16[16,2,1,22,256]{4,1,3,2,0:T(2,128)(2,1)}), bf16[16,2,1,22,256]{4,1,3,2,0:T(2,128)(2,1)S(1)}, u32[]{:S(2)}, u32[]{:S(2)}) async-start(bf16[16,2,1,22,256]{4,1,3,2,0:T(2,128)(2,1)} %copy.46), calls=%async_computation.1 | async-start | bytes 720896 | tf_op jit(solution)/shard_map/all_to_all | solution.py:39
  42.1 131.8 %all-gather.6.cloned.1.call-start = ((), (), s32[]{:S(2)}) async-start(), calls=%async_computation.4 | async-start | bytes 6127616 | tf_op jit(solution)/shard_map/all_gather | solution.py:163
  64.0 190.1 %all-gather.8.cloned.1.call-start = ((), (), s32[]{:S(2)}) async-start(), calls=%async_computation.5 | async-start | bytes 4177920 | tf_op jit(solution)/shard_map/all_gather | solution.py:20
  131.2 46.7 %copy-start.7 = (f32[4096]{0:T(1024)S(1)}, f32[4096]{0:T(1024)}, u32[]{:S(2)}) copy-start(f32[4096]{0:T(1024)} %param.24) | copy-start | bytes 49156
  173.9 4.3 %copy-start.1 = (bf16[704,4096]{1,0:T(8,128)(2,1)S(1)}, bf16[704,4096]{1,0:T(8,128)(2,1)}, u32[]{:S(2)}) copy-start(bf16[704,4096]{1,0:T(8,128)(2,1)} %all-gather.6.cloned.1.call-done) | copy-start | bytes 17301508
  178.2 3.0 copy-start.5
  183.7 88.5 %copy-start.3 = (f32[256,2]{0,1:T(2,128)S(1)}, f32[256,2]{0,1:T(2,128)}, u32[]{:S(2)}) copy-start(f32[256,2]{0,1:T(2,128)} %param.26) | copy-start | bytes 6148
  183.7 90.1 %copy-start.6 = (bf16[2048,256]{1,0:T(8,128)(2,1)S(1)}, bf16[2048,256]{1,0:T(8,128)(2,1)}, u32[]{:S(2)}) copy-start(bf16[2048,256]{1,0:T(8,128)(2,1)} %param.22) | copy-start | bytes 3145732
  183.7 90.1 %copy-start.8 = (f32[2048]{0:T(1024)S(1)}, f32[2048]{0:T(1024)}, u32[]{:S(2)}) copy-start(f32[2048]{0:T(1024)} %param.21) | copy-start | bytes 24580
  257.8 42.1 %all-to-all-start.2 = ((bf16[32,22,256]{2,1,0:T(8,128)(2,1)}), bf16[32,22,256]{2,1,0:T(8,128)(2,1)S(1)}, u32[]{:S(2)}, u32[]{:S(2)}) async-start(bf16[32,22,256]{2,1,0:T(8,128)(2,1)} %reshape.435), calls=%async_computation.2 | async-start | bytes 786432 | tf_op jit(solution)/shard_map/all_to_all | solution.py:188
Sparse Core Ops, SparseCore 0:
  10.9 88.5 all-gather.3
  102.5 71.3 all-gather.5
  183.8 70.3 all-gather.7
where the time goes:
time: 311 us; the launch traced here: 310 us
  waiting for transfers between devices  192 us (62%)
  matrix products  31.9 us (10%)
  starting transfers between devices  24.3 us (8%)
  local copies, waits for them, and re-layouts  20.2 us (6%)
  other arithmetic  16.7 us (5%)
  between operations  14.2 us (5%)
  blocking collectives  10.5 us (3%)
    all_gather x2, waiting for transfers between devices, in_one_piece(): filled = lax.all_gather(both, axis, axis=dim, tiled=True)  106 us
    all_gather x1, waiting for transfers between devices, shards(): lax.all_gather(arrived, 'tp', axis=1, tiled=True).astype(jnp.float32)  42.5 us
    all_to_all x1, waiting for transfers between devices, shards(): lax.all_to_all(expert_back, EP, split_axis=0, concat_axis=0, tiled=True)  23.7 us
    all_to_all x1, waiting for transfers between devices, exchange_in_order(): filled = lax.all_to_all(filled, axes[k], k, k, tiled=True)  20 us
    all_to_all x1, starting transfers between devices, shards(): lax.all_to_all(expert_back, EP, split_axis=0, concat_axis=0, tiled=True)  14.4 us
    dot_general x8, matrix products, absorb(): jnp.einsum('hgrn,nhd->rhgd', rounded, value_block, preferred_element_type...  11.1 us
    dot_general x8, matrix products, absorb(): jnp.einsum('rhgd,nhd->hgrn', query_heads, key_block, preferred_element_ty...  11 us
    all_to_all x1, blocking collectives, exchange_in_order(): filled = lax.all_to_all(filled, axes[k], k, k, tiled=True)  10.5 us
  transfers between devices with their start and end apart: 5, of which 5 were waited for; matrix products, arithmetic and copies ran while one was open for 16% of the time, Pallas kernels for 0%

commit v1 on v0

--- a/solution.py
+++ b/solution.py
@@ -12,6 +12,11 @@
 EP = ("ep_0", "ep_1")
 EPS = 1e-06
 THETA = 10000.0
+
+
+def tiled_gather(shard, axis, dim):
+    copies = jnp.concatenate([shard] * lax.axis_size(axis), axis=dim)
+    return lax.all_to_all(copies, axis, dim, dim, tiled=True)
 
 
 def in_one_piece(arrays, axis, dim, along):
@@ -160,7 +165,7 @@
     arrived = exchange_by_chip(outgoing, ("ep_0", "ep_1"), (1, 0), 0, 0).reshape(
         slot_total, width_local
     )
-    piece_float = lax.all_gather(arrived, "tp", axis=1, tiled=True).astype(jnp.float32)
+    piece_float = tiled_gather(arrived, "tp", 1).astype(jnp.float32)
     gain_piece = expert_gain
     scaled_piece = (piece_float * gain_piece).astype(jnp.bfloat16)
     gate_rows = expert_gate[0]

time: 311 us -> 295 us (0.949)
  waiting for transfers between devices: 192 us -> 166 us
  starting transfers between devices: 24.3 us -> 29.6 us
  local copies, waits for them, and re-layouts: 20.2 us -> 23.6 us
    all_gather x1 -> x0, waiting for transfers between devices: 42.5 us -> none  [shards(): lax.all_gather(arrived, 'tp', axis=1, tiled=True).astype(jnp.float32)]
    all_to_all x0 -> x1, waiting for transfers between devices: none -> 9.39 us  [tiled_gather(): return lax.all_to_all(copies, axis, dim, dim, tiled=True)]
    all_gather x2, waiting for transfers between devices: 106 us -> 113 us  [in_one_piece(): filled = lax.all_gather(both, axis, axis=dim, tiled=True)]
    all_to_all x0 -> x1, starting transfers between devices: none -> 5.37 us  [tiled_gather(): return lax.all_to_all(copies, axis, dim, dim, tiled=True)]
    concatenate x0 -> x2, local copies, waits for them, and re-layouts: none -> 3.22 us  [tiled_gather(): copies = jnp.concatenate([shard] * lax.axis_size(axis), axis=dim)]
  transfers between devices with their start and end apart: 5 -> 5, of which waited for: 5 -> 5; matrix products, arithmetic and copies ran while one was open for 16% -> 17% of each run, Pallas kernels for 0% -> 0%
where the time goes in v1:
time: 295 us; the launch traced here: 294 us
  waiting for transfers between devices  166 us (56%)
  matrix products  30.5 us (10%)
  starting transfers between devices  29.6 us (10%)
  local copies, waits for them, and re-layouts  23.6 us (8%)
  other arithmetic  19.3 us (7%)
  between operations  14.5 us (5%)
  blocking collectives  10.5 us (4%)
    all_gather x2, waiting for transfers between devices, in_one_piece(): filled = lax.all_gather(both, axis, axis=dim, tiled=True)  113 us
    all_to_all x1, waiting for transfers between devices, shards(): lax.all_to_all(expert_back, EP, split_axis=0, concat_axis=0, tiled=True)  23.6 us
    all_to_all x1, waiting for transfers between devices, exchange_in_order(): filled = lax.all_to_all(filled, axes[k], k, k, tiled=True)  19.9 us
    all_to_all x1, starting transfers between devices, shards(): lax.all_to_all(expert_back, EP, split_axis=0, concat_axis=0, tiled=True)  14.4 us
    dot_general x8, matrix products, absorb(): jnp.einsum('hgrn,nhd->rhgd', rounded, value_block, preferred_element_type...  11.1 us
    dot_general x8, matrix products, absorb(): jnp.einsum('rhgd,nhd->hgrn', query_heads, key_block, preferred_element_ty...  11 us
    all_to_all x1, blocking collectives, exchange_in_order(): filled = lax.all_to_all(filled, axes[k], k, k, tiled=True)  10.5 us
    all_to_all x1, starting transfers between devices, exchange_in_order(): filled = lax.all_to_all(filled, axes[k], k, k, tiled=True)  9.57 us
  transfers between devices with their start and end apart: 5, of which 5 were waited for; matrix products, arithmetic and copies ran while one was open for 17% of the time, Pallas kernels for 0%

profile of v1, /device:TPU:1, one launch (start us, length us, event | category | flops | bytes accessed | tf_op | source)
XLA Modules:
  0.0 294.3 jit_solution(8911861369216282384)
XLA Ops:
  9.4 1.4 pad_maximum_fusion.1
  15.4 2.4 scatter_custom_fusion
  17.9 2.8 gather_fusion
  20.9 10.5 %all_to_all.21 = bf16[16,2,1,22,256]{4,0,3,2,1:T(8,128)(2,1)S(1)} all-to-all(bf16[16,2,1,22,256]{4,0,3,2,1:T(8,128)(2,1)S(1)} %copy.61), channel_id=1, replica_groups=mesh['ep_0'=16,'ep_1'=2,'tp'=16] {'ep_1'}, dimensions={1} | all-to-all | bytes 720896 | tf_op jit(solution)/shard_map/all_to_all | solution.py:44
  32.5 9.6 %all-to-all-start.1 = ((bf16[16,2,1,22,256]{4,1,3,2,0:T(2,128)(2,1)}), bf16[16,2,1,22,256]{4,1,3,2,0:T(2,128)(2,1)S(1)}, u32[]{:S(2)}, u32[]{:S(2)}) async-start(bf16[16,2,1,22,256]{4,1,3,2,0:T(2,128)(2,1)} %copy.62), calls=%async_computation.1 | async-start | bytes 720896 | tf_op jit(solution)/shard_map/all_to_all | solution.py:44
  43.1 19.9 %all-to-all-done.1 = bf16[16,2,1,22,256]{4,1,3,2,0:T(2,128)(2,1)S(1)} async-done(((bf16[16,2,1,22,256]{4,1,3,2,0:T(2,128)(2,1)}), bf16[16,2,1,22,256]{4,1,3,2,0:T(2,128)(2,1)S(1)}, u32[]{:S(2)}, u32[]{:S(2)}) %all-to-all-start.1) | async-done | bytes 360480 | tf_op jit(solution)/shard_map/all_to_all | solution.py:44
  63.2 3.1 %concatenate.55 = bf16[704,16,256]{2,0,1:T(8,128)(2,1)} broadcast(bf16[704,256]{1,0:T(8,128)(2,1)S(1)} %concatenate.54), dimensions={0,2} | broadcast | bytes 6127616 | tf_op jit(solution)/shard_map/concatenate | solution.py:18
  66.3 5.4 %all-to-all-start.2 = ((bf16[704,16,256]{2,0,1:T(8,128)(2,1)}), bf16[704,16,256]{2,0,1:T(8,128)(2,1)}, u32[]{:S(2)}, u32[]{:S(2)}) async-start(bf16[704,16,256]{2,0,1:T(8,128)(2,1)} %concatenate.55), calls=%async_computation.2 | async-start | bytes 11534336 | tf_op jit(solution)/shard_map/all_to_all | solution.py:19
  71.9 27.6 %all-gather.3.cloned.1.call-done = bf16[8192,128]{0,1:T(8,128)(2,1)} async-done(((bf16[256,128]{0,1:T(8,128)(2,1)}), bf16[8192,128]{0,1:T(8,128)(2,1)}) %all-gather.3.cloned.1.call-update) | async-done | bytes 2097168 | tf_op jit(solution)/shard_map/all_gather | solution.py:25
  99.5 1.7 fusion.57
  101.8 1.5 copy.55
  104.0 1.6 copy.56
  105.6 25.6 %while.15 = (s32[]{:T(128)}, f32[1,2,256]{2,1,0:T(2,128)S(1)}, f32[1,2,256]{2,1,0:T(2,128)S(1)}, f32[256,1,2,64]{0,3,2,1:T(8,128)S(1)}, bf16[8,1024,1,64]{1,3,2,...) while((s32[]{:T(128)}, f32[1,2,256]{2,1,0:T(2,128)S(1)}, ...), condition=%wide.region_5.6_spmd.clone, body=%wide.region_2.5_spmd.clone.sunk | while | flops 138513408 | bytes 6914169 | solution.py:140
  131.4 9.4 %all-to-all-done.2 = bf16[704,16,256]{2,0,1:T(8,128)(2,1)} async-done(((bf16[704,16,256]{2,0,1:T(8,128)(2,1)}), bf16[704,16,256]{2,0,1:T(8,128)(2,1)}, u32[]{:S(2)}, u32[]{:S(2)}) %all-to-all-start.2) | async-done | bytes 5767200 | tf_op jit(solution)/shard_map/all_to_all | solution.py:19
  140.8 6.5 %fusion.19 = (f32[704]{0:T(1024)S(1)}, bf16[16,88,8,256]{3,2,1,0:T(8,128)(2,1)S(1)}) fusion(bf16[704,16,256]{2,0,1:T(8,128)(2,1)} %all-to-all-done.2, f32[16,256]{1,0:T(8,128)S(1)} %mul.300), kind=kLoop, calls=%fused_computation.32 | loop fusion | flops 14417216 | bytes 11553536 | tf_op jit(solution)/shard_map/reduce_sum | solution.py:175
  148.5 1.7 convolution_multiply_fusion.1
  150.2 1.7 fusion.29
  152.7 85.4 %all-gather.5.cloned.1.call-done = bf16[960,2048]{1,0:T(8,128)(2,1)} async-done(((bf16[960,128]{1,0:T(8,128)(2,1)}), bf16[960,2048]{1,0:T(8,128)(2,1)}) %all-gather.5.cloned.1.call-update) | async-done | bytes 3932176 | tf_op jit(solution)/shard_map/all_gather | solution.py:25
  238.1 2.7 fusion.25
  241.7 14.4 %all-to-all-start.3 = ((bf16[32,22,256]{2,1,0:T(8,128)(2,1)}), bf16[32,22,256]{2,1,0:T(8,128)(2,1)S(1)}, u32[]{:S(2)}, u32[]{:S(2)}) async-start(bf16[32,22,256]{2,1,0:T(8,128)(2,1)} %reshape.482), calls=%async_computation.3 | async-start | bytes 786432 | tf_op jit(solution)/shard_map/all_to_all | solution.py:193
  256.2 1.5 fusion.24
  257.8 2.3 fusion.30
  260.1 23.6 %all-to-all-done.3 = bf16[32,22,256]{2,1,0:T(8,128)(2,1)S(1)} async-done(((bf16[32,22,256]{2,1,0:T(8,128)(2,1)}), bf16[32,22,256]{2,1,0:T(8,128)(2,1)S(1)}, u32[]{:S(2)}, u32[]{:S(2)}) %all-to-all-start.3) | async-done | bytes 360480 | tf_op jit(solution)/shard_map/all_to_all | solution.py:193
  283.9 2.0 gather_fusion.1
  (132 shorter events, 40.6 us)
Async XLA Ops:
  7.2 230.9 %copy-start = (bf16[1,2048,256]{2,1,0:T(8,128)(2,1)S(1)}, bf16[1,2048,256]{2,1,0:T(8,128)(2,1)}, u32[]{:S(2)}) copy-start(bf16[1,2048,256]{2,1,0:T(8,128)(2,1)} %param.29) | copy-start | bytes 3145732
  7.2 92.3 %all-gather.3.cloned.1.call-start = ((), (), s32[]{:S(2)}) async-start(), calls=%async_computation.4 | async-start | bytes 2162688 | tf_op jit(solution)/shard_map/all_gather | solution.py:25
  17.9 24.3 %copy-start.2 = (f32[4096]{0:T(1024)S(1)}, f32[4096]{0:T(1024)}, u32[]{:S(2)}) copy-start(f32[4096]{0:T(1024)} %param.24) | copy-start | bytes 49156
  17.9 24.3 %copy-start.1 = (bf16[256,128]{1,0:T(8,128)(2,1)S(1)}, bf16[256,128]{1,0:T(8,128)(2,1)}, u32[]{:S(2)}) copy-start(bf16[256,128]{1,0:T(8,128)(2,1)} %param.16) | copy-start | bytes 196612
  17.9 24.5 %copy-start.4 = (f32[64]{0:T(128)S(1)}, f32[64]{0:T(128)}, u32[]{:S(2)}) copy-start(f32[64]{0:T(128)} %param.19) | copy-start | bytes 772
  32.5 30.5 %all-to-all-start.1 = ((bf16[16,2,1,22,256]{4,1,3,2,0:T(2,128)(2,1)}), bf16[16,2,1,22,256]{4,1,3,2,0:T(2,128)(2,1)S(1)}, u32[]{:S(2)}, u32[]{:S(2)}) async-start(bf16[16,2,1,22,256]{4,1,3,2,0:T(2,128)(2,1)} %copy.62), calls=%async_computation.1 | async-start | bytes 720896 | tf_op jit(solution)/shard_map/all_to_all | solution.py:44
  66.3 74.5 %all-to-all-start.2 = ((bf16[704,16,256]{2,0,1:T(8,128)(2,1)}), bf16[704,16,256]{2,0,1:T(8,128)(2,1)}, u32[]{:S(2)}, u32[]{:S(2)}) async-start(bf16[704,16,256]{2,0,1:T(8,128)(2,1)} %concatenate.55), calls=%async_computation.2 | async-start | bytes 11534336 | tf_op jit(solution)/shard_map/all_to_all | solution.py:19
  71.7 166.4 %all-gather.5.cloned.1.call-start = ((), (), s32[]{:S(2)}) async-start(), calls=%async_computation.5 | async-start | bytes 4177920 | tf_op jit(solution)/shard_map/all_gather | solution.py:25
  147.3 1.2 copy-start.5
  148.5 1.7 copy-start.6
  152.6 103.4 %copy-start.3 = (f32[256,2]{0,1:T(2,128)S(1)}, f32[256,2]{0,1:T(2,128)}, u32[]{:S(2)}) copy-start(f32[256,2]{0,1:T(2,128)} %param.26) | copy-start | bytes 6148
  152.6 105.1 %copy-start.7 = (bf16[2048,256]{1,0:T(8,128)(2,1)S(1)}, bf16[2048,256]{1,0:T(8,128)(2,1)}, u32[]{:S(2)}) copy-start(bf16[2048,256]{1,0:T(8,128)(2,1)} %param.22) | copy-start | bytes 3145732
  152.6 105.1 %copy-start.8 = (f32[2048]{0:T(1024)S(1)}, f32[2048]{0:T(1024)}, u32[]{:S(2)}) copy-start(f32[2048]{0:T(1024)} %param.21) | copy-start | bytes 24580
  241.7 42.1 %all-to-all-start.3 = ((bf16[32,22,256]{2,1,0:T(8,128)(2,1)}), bf16[32,22,256]{2,1,0:T(8,128)(2,1)S(1)}, u32[]{:S(2)}, u32[]{:S(2)}) async-start(bf16[32,22,256]{2,1,0:T(8,128)(2,1)} %reshape.482), calls=%async_computation.3 | async-start | bytes 786432 | tf_op jit(solution)/shard_map/all_to_all | solution.py:193
Sparse Core Ops, SparseCore 0:
  10.9 88.5 all-gather.2
  152.7 85.3 all-gather.4
